TPU v7x, 32 devices: a whole 2x2x4 slice. The times are simulated.
32 devices in a mesh: ep: 32 (over z, y, x, core).
Axes of the slice: x: 2, y: 2, z: 4, core: 2. Of those that a mesh axis runs over, the one named last changes fastest.
Arguments:
- tokens: bfloat16 [768, 2048], P('ep'), may hold values from -6 to 6
- lengths: int32 [768], P('ep'), may hold values from 2 to 1024
- latent_cache: bfloat16 [768, 1024, 256], P('ep'), may hold values from -500 to 500
- rotary_cache: bfloat16 [768, 1024, 32], P('ep'), may hold values from -6 to 6
- route_ids: int32 [768, 6], P('ep'), may hold values from 0 to 31, all different within a row; in each aligned block of 24 rows (0 to 23, 24 to 47, ...) at most 12 rows name the same one
- route_scores: float32 [768, 6], P('ep'), may hold values from 0.05 to 1
- attn_gain: bfloat16 [2048], replicated, may hold values from 0.099609375 to 1.8984375
- w_query_down: bfloat16 [2048, 256], replicated, may hold values from -0.125 to 0.125
- query_gain: bfloat16 [256], replicated, may hold values from 0.099609375 to 1.8984375
- w_query_nope: bfloat16 [256, 2048], replicated, may hold values from -0.375 to 0.375
- w_query_rope: bfloat16 [256, 1024], replicated, may hold values from -0.375 to 0.375
- w_key_absorb: bfloat16 [32, 64, 256], replicated, may hold values from -0.75 to 0.75
- latent_gain: bfloat16 [256], replicated, may hold values from 0.099609375 to 1.8984375
- w_latent_down: bfloat16 [2048, 256], replicated, may hold values from -0.125 to 0.125
- w_rotary_key: bfloat16 [2048, 32], replicated, may hold values from -0.125 to 0.125
- w_value_up: bfloat16 [32, 256, 64], replicated, may hold values from -0.375 to 0.375
- w_output: bfloat16 [2048, 2048], P(None, 'ep'), may hold values from -0.125 to 0.125
- ffn_gain: bfloat16 [2048], replicated, may hold values from 0.099609375 to 1.8984375
- expert_gate: bfloat16 [32, 2048, 512], P('ep'), may hold values from -0.125 to 0.125
- expert_up: bfloat16 [32, 2048, 512], P('ep'), may hold values from -0.125 to 0.125
- expert_down: bfloat16 [32, 512, 2048], P('ep'), may hold values from -0.25 to 0.25
- shared_gate: bfloat16 [2048, 256], replicated, may hold values from -0.125 to 0.125
- shared_up: bfloat16 [2048, 256], replicated, may hold values from -0.125 to 0.125
- shared_down: bfloat16 [256, 2048], replicated, may hold values from -0.375 to 0.375
Outputs:
- mixed: bfloat16 [768, 2048], P('ep')
- latent_new: bfloat16 [768, 256], P('ep')
- rotary_new: bfloat16 [768, 32], P('ep')
Inputs may be any that keep to these rules, and one draw needn't show every extreme that they name: `route_ids`: within the rows of one device no expert is named by more than 12 rows, a bound that some block reaches; each row names 6 different experts. `lengths`: cache positions at or past a sequence's length are not read.
All inputs are finite; a program needn't handle non-finite values.
Results may differ from a plain program's by a relative error of at most 0.025.
Values may be sent and summed in bfloat16 or wider, within the bound.
A program may use at most 128 MiB of HBM per device.

v0:
```python
import jax
import jax.numpy as jnp
from jax import lax
from jax.sharding import PartitionSpec as P

EPSILON = 1e-06
THETA = 10000.0
ROUTED_SCALE = 2.5


def rms_scale(values, gain):
    squares = jnp.mean(values * values, axis=-1, keepdims=True)
    return values * lax.rsqrt(squares + EPSILON) * gain.astype(jnp.float32)


def rotate(values, positions):
    half = values.shape[-1] // 2
    freqs = 1.0 / THETA ** (jnp.arange(half, dtype=jnp.float32) * 2.0 / values.shape[-1])
    angles = positions.astype(jnp.float32)[:, None] * freqs[None, :]
    if values.ndim == 3:
        angles = angles[:, None, :]
    cosine, sine = (jnp.cos(angles), jnp.sin(angles))
    first, second = (values[..., :half], values[..., half:])
    return jnp.concatenate(
        [first * cosine - second * sine, second * cosine + first * sine], axis=-1
    )


def shards(
    tokens,
    lengths,
    latent_cache,
    rotary_cache,
    route_ids,
    route_scores,
    attn_gain,
    w_query_down,
    query_gain,
    w_query_nope,
    w_query_rope,
    w_key_absorb,
    latent_gain,
    w_latent_down,
    w_rotary_key,
    w_value_up,
    w_output,
    ffn_gain,
    expert_gate,
    expert_up,
    expert_down,
    shared_gate,
    shared_up,
    shared_down,
):
    f32 = jnp.float32
    bf16 = jnp.bfloat16
    rows, model = tokens.shape
    heads, nope, latent = w_key_absorb.shape
    rotary = w_rotary_key.shape[1]
    top = route_ids.shape[1]
    normed = rms_scale(tokens.astype(f32), attn_gain).astype(bf16)
    query_low = rms_scale(
        jnp.dot(normed, w_query_down, preferred_element_type=f32), query_gain
    ).astype(bf16)
    query_nope = (
        jnp.dot(query_low, w_query_nope, preferred_element_type=f32)
        .astype(bf16)
        .reshape(rows, heads, nope)
    )
    query_rot = jnp.dot(query_low, w_query_rope, preferred_element_type=f32).reshape(
        rows, heads, rotary
    )
    query_rot = rotate(query_rot, lengths).astype(bf16)
    query_lat = jnp.einsum(
        "thn,hnl->thl", query_nope, w_key_absorb, preferred_element_type=f32
    ).astype(bf16)
    latent_new = rms_scale(
        jnp.dot(normed, w_latent_down, preferred_element_type=f32), latent_gain
    ).astype(bf16)
    rotary_new = rotate(jnp.dot(normed, w_rotary_key, preferred_element_type=f32), lengths).astype(
        bf16
    )
    scale = (nope + rotary) ** (-0.5)
    scores = (
        jnp.einsum("thl,tkl->thk", query_lat, latent_cache, preferred_element_type=f32)
        + jnp.einsum("thr,tkr->thk", query_rot, rotary_cache, preferred_element_type=f32)
    ) * scale
    live = jnp.arange(latent_cache.shape[1], dtype=jnp.int32)[None, :] < lengths[:, None]
    scores = jnp.where(live[:, None, :], scores, -jnp.inf)
    own = (
        jnp.einsum("thl,tl->th", query_lat, latent_new, preferred_element_type=f32)
        + jnp.einsum("thr,tr->th", query_rot, rotary_new, preferred_element_type=f32)
    ) * scale
    highest = jnp.maximum(jnp.max(scores, axis=-1), own)
    weights = jnp.exp(scores - highest[..., None])
    own_weight = jnp.exp(own - highest)
    total = jnp.sum(weights, axis=-1) + own_weight
    probs = (weights / total[..., None]).astype(bf16)
    own_prob = (own_weight / total).astype(bf16)
    out_lat = jnp.einsum("thk,tkl->thl", probs, latent_cache, preferred_element_type=f32)
    out_lat = (
        out_lat + own_prob.astype(f32)[..., None] * latent_new.astype(f32)[:, None, :]
    ).astype(bf16)
    values = jnp.einsum("thl,hlv->thv", out_lat, w_value_up, preferred_element_type=f32).astype(
        bf16
    )
    values = values.reshape(rows, model)
    attended = jnp.dot(
        values, lax.all_gather(w_output, "ep", axis=1, tiled=True), preferred_element_type=f32
    ).astype(bf16)
    residual = (tokens.astype(f32) + attended.astype(f32)).astype(bf16)
    ffn_in = rms_scale(residual.astype(f32), ffn_gain).astype(bf16)
    devices = lax.axis_size("ep")
    local_experts = expert_gate.shape[0]
    experts = devices * local_experts
    capacity = max(2, rows * top * 8 // (3 * experts))
    flat_ids = route_ids.reshape(-1)
    hits = (flat_ids[:, None] == jnp.arange(experts, dtype=jnp.int32)[None, :]).astype(jnp.int32)
    earlier = jnp.cumsum(hits, axis=0) - hits
    slot = jnp.sum(earlier * hits, axis=1)
    target = flat_ids * capacity + slot
    slot_range = jnp.arange(experts * capacity, dtype=jnp.int32)
    per_token = jnp.any(
        slot_range[:, None, None] == target.reshape(rows, top)[None, :, :], axis=2
    ).astype(bf16)
    per_pair = (target[:, None] == slot_range[None, :]).astype(bf16)
    outgoing = (
        jnp.dot(per_token, ffn_in, preferred_element_type=f32)
        .astype(bf16)
        .reshape(experts, capacity, model)
    )
    arrived = lax.all_to_all(outgoing, "ep", split_axis=0, concat_axis=0, tiled=True)
    count = arrived.shape[1]
    grouped = arrived.reshape(devices, local_experts, count, model)
    gate = jnp.einsum("sjcd,jdf->sjcf", grouped, expert_gate, preferred_element_type=f32)
    upward = jnp.einsum("sjcd,jdf->sjcf", grouped, expert_up, preferred_element_type=f32)
    hidden = (jax.nn.silu(gate) * upward).astype(bf16)
    result = jnp.einsum("sjcf,jfd->sjcd", hidden, expert_down, preferred_element_type=f32).astype(
        bf16
    )
    returned = lax.all_to_all(
        result.reshape(devices * local_experts, count, model),
        "ep",
        split_axis=0,
        concat_axis=0,
        tiled=True,
    )
    picked = jnp.dot(
        per_pair, returned.reshape(experts * capacity, model), preferred_element_type=f32
    )
    route_weight = ROUTED_SCALE * route_scores / jnp.sum(route_scores, axis=1, keepdims=True)
    routed = jnp.sum(picked.reshape(rows, top, model) * route_weight[:, :, None], axis=1)
    gate_shared = jnp.dot(ffn_in, shared_gate, preferred_element_type=f32)
    up_shared = jnp.dot(ffn_in, shared_up, preferred_element_type=f32)
    hidden_shared = (jax.nn.silu(gate_shared) * up_shared).astype(bf16)
    shared_out = jnp.dot(hidden_shared, shared_down, preferred_element_type=f32)
    mixed = (residual.astype(f32) + routed + shared_out).astype(bf16)
    return (mixed, latent_new, rotary_new)


def solution(mesh):
    return jax.shard_map(
        shards,
        mesh=mesh,
        in_specs=(
            P("ep", None),
            P("ep"),
            P("ep", None, None),
            P("ep", None, None),
            P("ep", None),
            P("ep", None),
            P(),
            P(),
            P(),
            P(),
            P(),
            P(),
            P(),
            P(),
            P(),
            P(),
            P(None, "ep"),
            P(),
            P("ep", None, None),
            P("ep", None, None),
            P("ep", None, None),
            P(),
            P(),
            P(),
        ),
        out_specs=(P("ep", None), P("ep", None), P("ep", None)),
        check_vma=False,
    )
```

profile of v0, /device:TPU:0, one launch (start us, length us, event | category | flops | bytes accessed | tf_op | source)
XLA Modules:
  0.0 232.9 jit_solution(12893498353833350144)
XLA Ops:
  7.3 0.7 all-gather.2.cloned.1.call-update
  8.0 0.7 convert_element_type.102
  8.6 0.7 convert_element_type.104
  9.3 1.0 fusion.55
  10.3 1.7 multiply_reduce_fusion.2
  12.0 1.3 fusion.77
  13.3 0.2 reshape.207
  13.5 1.5 convolution_convert_fusion.2
  15.0 0.9 reshape.206
  15.9 0.2 fusion.80
  16.2 0.1 subtract_convert_fusion.1
  16.4 1.6 multiply_reduce_fusion.1
  18.0 0.2 subtract_convert_fusion
  18.2 0.3 fusion.62
  18.5 0.1 iota_compare_fusion.2
  18.7 0.3 fusion.32
  19.0 0.3 copy-done.10
  19.3 0.2 fusion.48
  19.5 8.8 %fusion.50 = f32[24,32,1024]{2,1,0:T(8,128)S(1)} fusion(bf16[24,1024,256]{2,1,0:T(8,128)(2,1)} %param.26, bf16[24,32,256]{2,0,1:T(8,128)(2,1)S(1)} %fusion.32), kind=kOutput, calls=%fused_computation.50 | convolution fusion | flops 402653184 | bytes 16121856 | tf_op jit(solution)/shard_map/thl,tkl->thk/dot_general | solution.py:85
  28.3 2.6 %fusion.87 = (f32[24,32]{1,0:T(8,128)S(1)}, f32[24,32,1024]{2,1,0:T(8,128)S(1)}) fusion(f32[24,32,1024]{2,1,0:T(8,128)S(1)} %fusion.50, bf16[24,1024,32]{1,2,0:T(8,128)(2,1)} %param.27, bf16[24,32,16]{2,1,0:T(8,128)(2,1)S(1)} %get-tuple-element.6, bf16[24,32,16]{2,1,0:T(8,128)(2,1)S(1)} %get-tuple-element.5, pred[24,1024]{1,0:T(8,128)(4,1)S(1)} %iota_compare_fusion.2), kind=kOutput, calls=%fused_computation.118 | convolution fusion | flops 53574912 | bytes 7941120 | tf_op jit(solution)/shard_map/thr,tkr->thk/dot_general | solution.py:86
  30.9 0.7 fusion
  31.6 2.1 fusion.28
  33.7 0.5 fusion.33
  34.2 0.2 reshape.208
  34.5 0.1 copy.72
  34.6 0.1 eq.64
  34.7 0.6 reduce-window.6
  35.3 0.2 slice_reduce_fusion
  35.6 0.1 reduce_sum.79
  35.7 0.1 copy.75
  35.8 0.1 fusion.54
  35.9 54.8 %all-gather.2.cloned.1.call-done = bf16[2048,2048]{0,1:T(8,128)(2,1)} async-done(((bf16[2048,64]{0,1:T(8,128)(2,1)}), bf16[2048,2048]{0,1:T(8,128)(2,1)}) %all-gather.2.cloned.1.call-update) | async-done | bytes 8388624 | tf_op jit(solution)/shard_map/all_gather | solution.py:109
  90.7 5.8 %multiply_reduce_fusion = (f32[24]{0:T(128)S(1)}, f32[24,2048]{1,0:T(8,128)S(1)}) fusion(bf16[24,2048]{1,0:T(8,128)(2,1)S(1)} %reshape.208, bf16[2048,2048]{0,1:T(8,128)(2,1)} %all-gather.2.cloned.1.call-done, bf16[24,2048]{1,0:T(8,128)(2,1)S(1)} %copy-done.2), kind=kOutput, calls=%fused_computation.64 | convolution fusion | flops 201719776 | bytes 8781920 | tf_op jit(solution)/shard_map/dot_general | solution.py:108
  96.5 1.8 convolution_convert_fusion
  98.3 3.6 %reshape.211 = bf16[32,12,2048]{2,1,0:T(8,128)(2,1)} reshape(bf16[384,2048]{1,0:T(8,128)(2,1)} %convolution_convert_fusion) | data formatting | bytes 3145728 | tf_op jit(solution)/shard_map/reshape | solution.py:130
  101.9 51.9 %all_to_all.10 = bf16[32,12,2048]{2,1,0:T(8,128)(2,1)S(1)} all-to-all(bf16[32,12,2048]{2,1,0:T(8,128)(2,1)} %reshape.211), channel_id=1, replica_groups=mesh['ep'=32] {'ep'}, dimensions={0} | all-to-all | bytes 3145728 | tf_op jit(solution)/shard_map/all_to_all | solution.py:132
  153.8 1.3 copy-done.1
  155.2 1.1 fusion.14
  156.3 5.5 %convolution_convert_fusion.1 = bf16[32,12,2048]{2,0,1:T(8,128)(2,1)} fusion(bf16[1,512,2048]{2,1,0:T(8,128)(2,1)S(1)} %copy-done, bf16[1,2048,512]{2,1,0:T(8,128)(2,1)} %param.43, bf16[32,12,2048]{2,1,0:T(8,128)(2,1)} %copy-done.1, f32[32,1,12,512]{3,0,2,1:T(8,128)S(1)} %fusion.14), kind=kOutput, calls=%fused_computation.4 | convolution fusion | flops 1612578816 | bytes 8126464 | tf_op jit(solution)/shard_map/sjcf,jfd->sjcd/dot_general | solution.py:138
  161.7 3.6 %copy.78 = bf16[32,12,2048]{2,1,0:T(8,128)(2,1)} copy(bf16[32,12,2048]{2,0,1:T(8,128)(2,1)} %convolution_convert_fusion.1) | data formatting | bytes 3145728 | tf_op jit(solution)/shard_map/convert_element_type | solution.py:138
  165.3 3.8 %all-to-all-start.1 = ((bf16[32,12,2048]{2,1,0:T(8,128)(2,1)}), bf16[32,12,2048]{2,1,0:T(8,128)(2,1)}, u32[]{:S(2)}, u32[]{:S(2)}) async-start(bf16[32,12,2048]{2,1,0:T(8,128)(2,1)} %copy.78), calls=%async_computation.1 | async-start | bytes 4194304 | tf_op jit(solution)/shard_map/all_to_all | solution.py:141
  169.1 0.7 pad_maximum_fusion.3
  169.8 0.6 multiply_divide_fusion
  170.4 0.9 fusion.79
  171.3 46.5 %all-to-all-done.1 = bf16[32,12,2048]{2,1,0:T(8,128)(2,1)} async-done(((bf16[32,12,2048]{2,1,0:T(8,128)(2,1)}), bf16[32,12,2048]{2,1,0:T(8,128)(2,1)}, u32[]{:S(2)}, u32[]{:S(2)}) %all-to-all-start.1) | async-done | bytes 1572896 | tf_op jit(solution)/shard_map/all_to_all | solution.py:141
  217.8 3.6 %reshape.225 = bf16[384,2048,1]{1,0,2:T(8,128)(2,1)} reshape(bf16[32,12,2048]{2,1,0:T(8,128)(2,1)} %all-to-all-done.1) | data formatting | bytes 3145728 | tf_op jit(solution)/shard_map/reshape | solution.py:149
  221.4 1.9 fusion.24
  223.4 2.7 %fusion.1 = bf16[24,2048]{1,0:T(8,128)(2,1)} fusion(bf16[256,2048]{1,0:T(8,128)(2,1)S(1)} %copy-done.6, bf16[2048,256]{1,0:T(8,128)(2,1)} %param.46, f32[24,2048]{1,0:T(8,128)S(1)} %get-tuple-element.20, f32[24,2048]{1,0:T(8,128)S(1)} %fusion.24, f32[24,256]{1,0:T(8,128)} %fusion.79, f32[2048]{0:T(1024)S(1)} %convert_element_type.124, f32[24]{0:T(128)S(1)} %add_rsqrt_fusion), kind=kOutput, calls=%fused_computation.8 | convolution fusion | flops 50663424 | bytes 2621536 | tf_op jit(solution)/shard_map/dot_general | solution.py:156
  (59 shorter events, 0.6 us)
Async XLA Ops:
  7.2 149.1 %copy-start = (bf16[1,512,2048]{2,1,0:T(8,128)(2,1)S(1)}, bf16[1,512,2048]{2,1,0:T(8,128)(2,1)}, u32[]{:S(2)}) copy-start(bf16[1,512,2048]{2,1,0:T(8,128)(2,1)} %param.44) | copy-start | bytes 6291460
  7.2 8.7 %copy-start.2 = (bf16[24,2048]{1,0:T(8,128)(2,1)S(1)}, bf16[24,2048]{1,0:T(8,128)(2,1)}, u32[]{:S(2)}) copy-start(bf16[24,2048]{1,0:T(8,128)(2,1)} %param.24) | copy-start | bytes 294916
  7.2 6.3 %copy-start.12 = (s32[24]{0:T(128)S(1)}, s32[24]{0:T(128)}, u32[]{:S(2)}) copy-start(s32[24]{0:T(128)} %param.25) | copy-start | bytes 292
  7.2 8.7 %copy-start.15 = (bf16[256]{0:T(256)(128)(2,1)S(1)}, bf16[256]{0:T(256)(128)(2,1)}, u32[]{:S(2)}) copy-start(bf16[256]{0:T(256)(128)(2,1)} %param.36) | copy-start | bytes 1540
  7.2 8.7 %copy-start.14 = (bf16[2048,32]{0,1:T(8,128)(2,1)S(1)}, bf16[2048,32]{0,1:T(8,128)(2,1)}, u32[]{:S(2)}) copy-start(bf16[2048,32]{0,1:T(8,128)(2,1)} %param.38) | copy-start | bytes 393220
  7.2 83.5 %all-gather.2.cloned.1.call-start = ((), (), s32[]{:S(2)}) async-start(), calls=%async_computation.2 | async-start | bytes 8650752 | tf_op jit(solution)/shard_map/all_gather | solution.py:109
  15.9 2.8 %copy-start.3 = (bf16[32,64,256]{2,1,0:T(8,128)(2,1)S(1)}, bf16[32,64,256]{2,1,0:T(8,128)(2,1)}, u32[]{:S(2)}) copy-start(bf16[32,64,256]{2,1,0:T(8,128)(2,1)} %param.35) | copy-start | bytes 3145732
  15.9 2.8 %copy-start.7 = (bf16[24,32,64]{2,1,0:T(8,128)(2,1)S(1)}, bf16[24,32,64]{2,1,0:T(8,128)(2,1)}, u32[]{:S(2)}) copy-start(bf16[24,32,64]{2,1,0:T(8,128)(2,1)} %reshape.206) | copy-start | bytes 294916
  18.7 0.6 copy-start.10
  19.5 12.1 %slice-start = ((s8[12582912]{0:T(1024)(128)(4,1)}), s8[4194304]{0:T(1024)(128)(4,1)S(1)}, s32[]{:S(2)}) async-start(s8[12582912]{0:T(1024)(128)(4,1)} %bitcast.91), calls=%async_computation.3 | async-start | bytes 8388608
  19.5 12.1 %slice-start.1 = ((s8[12582912]{0:T(1024)(128)(4,1)}), s8[4194304]{0:T(1024)(128)(4,1)S(1)}, s32[]{:S(2)}) async-start(s8[12582912]{0:T(1024)(128)(4,1)} %bitcast.91), calls=%async_computation.4 | async-start | bytes 8388608
  28.3 3.3 %slice-start.2 = ((s8[12582912]{0:T(1024)(128)(4,1)}), s8[4194304]{0:T(1024)(128)(4,1)S(1)}, s32[]{:S(2)}) async-start(s8[12582912]{0:T(1024)(128)(4,1)} %bitcast.91), calls=%async_computation.5 | async-start | bytes 8388608
  31.6 2.1 copy-start.4
  33.7 0.8 copy-start.9
  33.7 2.1 copy-start.11
  101.9 53.3 %copy-start.13 = (bf16[1,2048,512]{2,1,0:T(8,128)(2,1)S(1)}, bf16[1,2048,512]{2,1,0:T(8,128)(2,1)}, u32[]{:S(2)}) copy-start(bf16[1,2048,512]{2,1,0:T(8,128)(2,1)} %param.42) | copy-start | bytes 6291460
  153.8 1.4 copy-start.1
  165.3 3.8 %copy-start.8 = (f32[24,6]{0,1:T(8,128)S(1)}, f32[24,6]{0,1:T(8,128)}, u32[]{:S(2)}) copy-start(f32[24,6]{0,1:T(8,128)} %param.29) | copy-start | bytes 1732
  165.3 5.1 %copy-start.5 = (bf16[2048,256]{1,0:T(8,128)(2,1)S(1)}, bf16[2048,256]{1,0:T(8,128)(2,1)}, u32[]{:S(2)}) copy-start(bf16[2048,256]{1,0:T(8,128)(2,1)} %param.45) | copy-start | bytes 3145732
  165.3 52.5 %all-to-all-start.1 = ((bf16[32,12,2048]{2,1,0:T(8,128)(2,1)}), bf16[32,12,2048]{2,1,0:T(8,128)(2,1)}, u32[]{:S(2)}, u32[]{:S(2)}) async-start(bf16[32,12,2048]{2,1,0:T(8,128)(2,1)} %copy.78), calls=%async_computation.1 | async-start | bytes 4194304 | tf_op jit(solution)/shard_map/all_to_all | solution.py:141
  171.3 52.1 %copy-start.6 = (bf16[256,2048]{1,0:T(8,128)(2,1)S(1)}, bf16[256,2048]{1,0:T(8,128)(2,1)}, u32[]{:S(2)}) copy-start(bf16[256,2048]{1,0:T(8,128)(2,1)} %param.47) | copy-start | bytes 3145732
Sparse Core Ops, SparseCore 0:
  10.9 79.7 all-gather.1
where the time goes:
time: 234 us; the launch traced here: 233 us
  waiting for transfers between devices  102 us (44%)
  blocking collectives  51.9 us (22%)
  matrix products  40.6 us (17%)
  local copies, waits for them, and re-layouts  14.4 us (6%)
  between operations  14.4 us (6%)
  other arithmetic  5.86 us (3%)
  starting transfers between devices  3.82 us (2%)
    all_gather x1, waiting for transfers between devices, shards(): lax.all_gather(w_output, 'ep', axis=1, tiled=True)  54.8 us
    all_to_all x1, blocking collectives, shards(): lax.all_to_all(outgoing, 'ep', split_axis=0, concat_axis=0, tiled=True)  51.9 us
    all_to_all x1, waiting for transfers between devices, shards(): lax.all_to_all(result.reshape(devices * local_experts, count, model), 'ep...  46.5 us
    dot_general x1, matrix products, shards(): jnp.einsum('thl,tkl->thk', query_lat, latent_cache, preferred_element_typ...  8.77 us
    dot_general x1, matrix products, shards(): jnp.dot(values, lax.all_gather(w_output, 'ep', axis=1, tiled=True), prefe...  5.77 us
    dot_general x1, matrix products, shards(): jnp.einsum('sjcf,jfd->sjcd', hidden, expert_down, preferred_element_type=...  5.45 us
  transfers between devices with their start and end apart: 2, of which 2 were waited for; matrix products, arithmetic and copies ran while one was open for 13% of the time, Pallas kernels for 0%

commit v1 on v0

--- a/solution.py
+++ b/solution.py
@@ -106,7 +106,11 @@
     )
     values = values.reshape(rows, model)
     attended = jnp.dot(
-        values, lax.all_gather(w_output, "ep", axis=1, tiled=True), preferred_element_type=f32
+        values,
+        jnp.concatenate(
+            lax.all_to_all(jnp.stack([w_output] * lax.axis_size("ep")), "ep", 0, 0), axis=1
+        ),
+        preferred_element_type=f32,
     ).astype(bf16)
     residual = (tokens.astype(f32) + attended.astype(f32)).astype(bf16)
     ffn_in = rms_scale(residual.astype(f32), ffn_gain).astype(bf16)

time: 234 us -> 335 us (1.43)
  waiting for transfers between devices: 102 us -> 208 us
  between operations: 14.4 us -> 1.06 us
  starting transfers between devices: 3.82 us -> 11.2 us
  local copies, waits for them, and re-layouts: 14.4 us -> 19.8 us
    all_to_all x0 -> x1, waiting for transfers between devices: none -> 161 us  [shards(): lax.all_to_all(jnp.stack([w_output] * lax.axis_size('ep')), 'ep', 0, 0)]
    all_gather x1 -> x0, waiting for transfers between devices: 54.8 us -> none  [shards(): lax.all_gather(w_output, 'ep', axis=1, tiled=True)]
    all_to_all x0 -> x1, starting transfers between devices: none -> 7.46 us  [shards(): lax.all_to_all(jnp.stack([w_output] * lax.axis_size('ep')), 'ep', 0, 0)]
    another operation x1 -> x2, local copies, waits for them, and re-layouts: 0.01 us -> 5.38 us  [the longest x1 5.37 us: shards(): jnp.stack([w_output] * lax.axis_size('ep'))]
  transfers between devices with their start and end apart: 2 -> 2, of which waited for: 2 -> 2; matrix products, arithmetic and copies ran while one was open for 13% -> 8% of each run, Pallas kernels for 0% -> 0%
where the time goes in v1:
time: 335 us; the launch traced here: 334 us
  waiting for transfers between devices  208 us (62%)
  blocking collectives  51.5 us (15%)
  matrix products  39.2 us (12%)
  local copies, waits for them, and re-layouts  19.8 us (6%)
  starting transfers between devices  11.2 us (3%)
  other arithmetic  3.63 us (1%)
    all_to_all x1, waiting for transfers between devices, shards(): lax.all_to_all(jnp.stack([w_output] * lax.axis_size('ep')), 'ep', 0, 0)  161 us
    all_to_all x1, blocking collectives, shards(): lax.all_to_all(outgoing, 'ep', split_axis=0, concat_axis=0, tiled=True)  51.5 us
    all_to_all x1, waiting for transfers between devices, shards(): lax.all_to_all(result.reshape(devices * local_experts, count, model), 'ep...  46.5 us
    dot_general x1, matrix products, shards(): jnp.einsum('thl,tkl->thk', query_lat, latent_cache, preferred_element_typ...  8.47 us
    all_to_all x1, starting transfers between devices, shards(): lax.all_to_all(jnp.stack([w_output] * lax.axis_size('ep')), 'ep', 0, 0)  7.46 us
  transfers between devices with their start and end apart: 2, of which 2 were waited for; matrix products, arithmetic and copies ran while one was open for 8% of the time, Pallas kernels for 0%

profile of v1, /device:TPU:0, one launch (start us, length us, event | category | flops | bytes accessed | tf_op | source)
XLA Modules:
  0.0 334.3 jit_solution(18199005317766984877)
XLA Ops:
  0.6 5.4 %stack.2 = bf16[32,2048,64]{1,2,0:T(8,128)(2,1)} broadcast(bf16[2048,64]{0,1:T(8,128)(2,1)} %param.40), dimensions={1,2} | broadcast | bytes 8650752 | tf_op jit(solution)/shard_map/stack | solution.py:111
  6.0 7.5 %all-to-all-start = ((bf16[32,2048,64]{1,2,0:T(8,128)(2,1)}), bf16[32,2048,64]{1,2,0:T(8,128)(2,1)}, u32[]{:S(2)}, u32[]{:S(2)}) async-start(bf16[32,2048,64]{1,2,0:T(8,128)(2,1)} %stack.2), calls=%async_computation | async-start | bytes 16777216 | tf_op jit(solution)/shard_map/all_to_all | solution.py:111
  13.6 0.1 fusion.55
  13.7 1.6 multiply_reduce_fusion.2
  15.4 0.2 fusion.77
  15.6 0.2 reshape.215
  15.8 1.5 convolution_convert_fusion.2
  17.3 0.9 reshape.214
  18.2 0.2 fusion.80
  18.4 0.1 subtract_convert_fusion.1
  18.6 0.1 fusion.105
  18.7 1.6 multiply_reduce_fusion.1
  20.3 0.2 subtract_convert_fusion
  20.5 0.3 fusion.62
  20.8 0.1 iota_compare_fusion.2
  21.0 0.3 fusion.32
  21.3 0.3 copy-done.11
  21.6 0.2 fusion.48
  21.8 8.5 %fusion.50 = f32[24,32,1024]{2,1,0:T(8,128)S(1)} fusion(bf16[24,1024,256]{2,1,0:T(8,128)(2,1)} %param.26, bf16[24,32,256]{2,0,1:T(8,128)(2,1)S(1)} %fusion.32), kind=kOutput, calls=%fused_computation.50 | convolution fusion | flops 402653184 | bytes 16121856 | tf_op jit(solution)/shard_map/thl,tkl->thk/dot_general | solution.py:85
  30.3 2.6 fusion.87
  32.9 0.7 fusion
  33.6 2.1 fusion.28
  35.7 0.5 fusion.33
  36.2 0.2 reshape.216
  36.5 0.1 copy.73
  36.6 0.1 eq.64
  36.7 0.6 reduce-window.6
  37.3 0.2 slice_reduce_fusion
  37.6 0.1 reduce_sum.79
  37.7 0.1 copy.76
  37.8 0.1 fusion.54
  37.9 161.5 %all-to-all-done = bf16[32,2048,64]{1,2,0:T(8,128)(2,1)} async-done(((bf16[32,2048,64]{1,2,0:T(8,128)(2,1)}), bf16[32,2048,64]{1,2,0:T(8,128)(2,1)}, u32[]{:S(2)}, u32[]{:S(2)}) %all-to-all-start) | async-done | bytes 8388640 | tf_op jit(solution)/shard_map/all_to_all | solution.py:111
  199.4 5.8 %multiply_reduce_fusion = (f32[24]{0:T(128)S(1)}, f32[24,2048]{1,0:T(8,128)S(1)}) fusion(bf16[24,2048]{1,0:T(8,128)(2,1)S(1)} %reshape.216, bf16[2048,2048]{0,1:T(8,128)(2,1)} %bitcast.9, bf16[24,2048]{1,0:T(8,128)(2,1)S(1)} %copy-done.2), kind=kOutput, calls=%fused_computation.64 | convolution fusion | flops 201719776 | bytes 8781920 | tf_op jit(solution)/shard_map/dot_general | solution.py:108
  205.2 1.8 convolution_convert_fusion
  207.0 3.6 %reshape.221 = bf16[32,12,2048]{2,1,0:T(8,128)(2,1)} reshape(bf16[384,2048]{1,0:T(8,128)(2,1)} %convolution_convert_fusion) | data formatting | bytes 3145728 | tf_op jit(solution)/shard_map/reshape | solution.py:134
  210.6 51.5 %all_to_all.15 = bf16[32,12,2048]{2,1,0:T(8,128)(2,1)S(1)} all-to-all(bf16[32,12,2048]{2,1,0:T(8,128)(2,1)} %reshape.221), channel_id=1, replica_groups=mesh['ep'=32] {'ep'}, dimensions={0} | all-to-all | bytes 3145728 | tf_op jit(solution)/shard_map/all_to_all | solution.py:136
  262.1 1.3 copy-done.1
  263.5 1.1 fusion.14
  264.6 5.4 %convolution_convert_fusion.1 = bf16[32,12,2048]{2,0,1:T(8,128)(2,1)} fusion(bf16[1,512,2048]{2,1,0:T(8,128)(2,1)S(1)} %copy-done, bf16[1,2048,512]{2,1,0:T(8,128)(2,1)} %param.43, bf16[32,12,2048]{2,1,0:T(8,128)(2,1)} %copy-done.1, f32[32,1,12,512]{3,0,2,1:T(8,128)S(1)} %fusion.14), kind=kOutput, calls=%fused_computation.4 | convolution fusion | flops 1612578816 | bytes 8126464 | tf_op jit(solution)/shard_map/sjcf,jfd->sjcd/dot_general | solution.py:142
  270.0 3.6 %copy.79 = bf16[32,12,2048]{2,1,0:T(8,128)(2,1)} copy(bf16[32,12,2048]{2,0,1:T(8,128)(2,1)} %convolution_convert_fusion.1) | data formatting | bytes 3145728 | tf_op jit(solution)/shard_map/convert_element_type | solution.py:142
  273.6 3.7 %all-to-all-start.2 = ((bf16[32,12,2048]{2,1,0:T(8,128)(2,1)}), bf16[32,12,2048]{2,1,0:T(8,128)(2,1)}, u32[]{:S(2)}, u32[]{:S(2)}) async-start(bf16[32,12,2048]{2,1,0:T(8,128)(2,1)} %copy.79), calls=%async_computation.2 | async-start | bytes 4194304 | tf_op jit(solution)/shard_map/all_to_all | solution.py:145
  277.4 0.7 pad_maximum_fusion.3
  278.1 0.6 multiply_divide_fusion
  278.7 0.9 fusion.79
  279.6 46.5 %all-to-all-done.2 = bf16[32,12,2048]{2,1,0:T(8,128)(2,1)} async-done(((bf16[32,12,2048]{2,1,0:T(8,128)(2,1)}), bf16[32,12,2048]{2,1,0:T(8,128)(2,1)}, u32[]{:S(2)}, u32[]{:S(2)}) %all-to-all-start.2) | async-done | bytes 1572896 | tf_op jit(solution)/shard_map/all_to_all | solution.py:145
  326.1 3.6 %reshape.235 = bf16[384,2048,1]{1,0,2:T(8,128)(2,1)} reshape(bf16[32,12,2048]{2,1,0:T(8,128)(2,1)} %all-to-all-done.2) | data formatting | bytes 3145728 | tf_op jit(solution)/shard_map/reshape | solution.py:153
  329.7 1.9 fusion.24
  331.6 2.7 fusion.1
  (65 shorter events, 0.5 us)
Async XLA Ops:
  0.6 263.9 %copy-start = (bf16[1,512,2048]{2,1,0:T(8,128)(2,1)S(1)}, bf16[1,512,2048]{2,1,0:T(8,128)(2,1)}, u32[]{:S(2)}) copy-start(bf16[1,512,2048]{2,1,0:T(8,128)(2,1)} %param.44) | copy-start | bytes 6291460
  6.0 7.5 %copy-start.12 = (bf16[2048]{0:T(1024)(128)(2,1)S(1)}, bf16[2048]{0:T(1024)(128)(2,1)}, u32[]{:S(2)}) copy-start(bf16[2048]{0:T(1024)(128)(2,1)} %param.30) | copy-start | bytes 12292
  6.0 7.5 %copy-start.17 = (bf16[256]{0:T(256)(128)(2,1)S(1)}, bf16[256]{0:T(256)(128)(2,1)}, u32[]{:S(2)}) copy-start(bf16[256]{0:T(256)(128)(2,1)} %param.32) | copy-start | bytes 1540
  6.0 7.6 %copy-start.2 = (bf16[24,2048]{1,0:T(8,128)(2,1)S(1)}, bf16[24,2048]{1,0:T(8,128)(2,1)}, u32[]{:S(2)}) copy-start(bf16[24,2048]{1,0:T(8,128)(2,1)} %param.24) | copy-start | bytes 294916
  6.0 9.4 %copy-start.8 = (bf16[256,1024]{1,0:T(8,128)(2,1)S(1)}, bf16[256,1024]{1,0:T(8,128)(2,1)}, u32[]{:S(2)}) copy-start(bf16[256,1024]{1,0:T(8,128)(2,1)} %param.34) | copy-start | bytes 1572868
  6.0 193.4 %all-to-all-start = ((bf16[32,2048,64]{1,2,0:T(8,128)(2,1)}), bf16[32,2048,64]{1,2,0:T(8,128)(2,1)}, u32[]{:S(2)}, u32[]{:S(2)}) async-start(bf16[32,2048,64]{1,2,0:T(8,128)(2,1)} %stack.2), calls=%async_computation | async-start | bytes 16777216 | tf_op jit(solution)/shard_map/all_to_all | solution.py:111
  13.5 2.3 copy-start.14
  13.5 4.7 %copy-start.18 = (bf16[256]{0:T(256)(128)(2,1)S(1)}, bf16[256]{0:T(256)(128)(2,1)}, u32[]{:S(2)}) copy-start(bf16[256]{0:T(256)(128)(2,1)} %param.36) | copy-start | bytes 1540
  13.5 4.7 %copy-start.16 = (bf16[2048,32]{0,1:T(8,128)(2,1)S(1)}, bf16[2048,32]{0,1:T(8,128)(2,1)}, u32[]{:S(2)}) copy-start(bf16[2048,32]{0,1:T(8,128)(2,1)} %param.38) | copy-start | bytes 393220
  18.2 2.8 copy-start.3
  18.2 2.8 copy-start.7
  21.0 0.6 copy-start.11
  21.8 11.8 %slice-start = ((s8[12582912]{0:T(1024)(128)(4,1)}), s8[4194304]{0:T(1024)(128)(4,1)S(1)}, s32[]{:S(2)}) async-start(s8[12582912]{0:T(1024)(128)(4,1)} %bitcast.94), calls=%async_computation.3 | async-start | bytes 8388608
  21.8 11.8 %slice-start.1 = ((s8[12582912]{0:T(1024)(128)(4,1)}), s8[4194304]{0:T(1024)(128)(4,1)S(1)}, s32[]{:S(2)}) async-start(s8[12582912]{0:T(1024)(128)(4,1)} %bitcast.94), calls=%async_computation.4 | async-start | bytes 8388608
  30.3 3.3 slice-start.2
  33.6 2.1 copy-start.4
  35.7 0.8 copy-start.13
  35.7 0.8 copy-start.10
  210.6 52.9 %copy-start.15 = (bf16[1,2048,512]{2,1,0:T(8,128)(2,1)S(1)}, bf16[1,2048,512]{2,1,0:T(8,128)(2,1)}, u32[]{:S(2)}) copy-start(bf16[1,2048,512]{2,1,0:T(8,128)(2,1)} %param.42) | copy-start | bytes 6291460
  262.1 1.4 copy-start.1
  273.6 3.7 %copy-start.9 = (f32[24,6]{0,1:T(8,128)S(1)}, f32[24,6]{0,1:T(8,128)}, u32[]{:S(2)}) copy-start(f32[24,6]{0,1:T(8,128)} %param.29) | copy-start | bytes 1732
  273.6 5.0 %copy-start.5 = (bf16[2048,256]{1,0:T(8,128)(2,1)S(1)}, bf16[2048,256]{1,0:T(8,128)(2,1)}, u32[]{:S(2)}) copy-start(bf16[2048,256]{1,0:T(8,128)(2,1)} %param.45) | copy-start | bytes 3145732
  273.6 52.4 %all-to-all-start.2 = ((bf16[32,12,2048]{2,1,0:T(8,128)(2,1)}), bf16[32,12,2048]{2,1,0:T(8,128)(2,1)}, u32[]{:S(2)}, u32[]{:S(2)}) async-start(bf16[32,12,2048]{2,1,0:T(8,128)(2,1)} %copy.79), calls=%async_computation.2 | async-start | bytes 4194304 | tf_op jit(solution)/shard_map/all_to_all | solution.py:145
  279.6 52.1 %copy-start.6 = (bf16[256,2048]{1,0:T(8,128)(2,1)S(1)}, bf16[256,2048]{1,0:T(8,128)(2,1)}, u32[]{:S(2)}) copy-start(bf16[256,2048]{1,0:T(8,128)(2,1)} %param.47) | copy-start | bytes 3145732
